TPU v7x, 32 devices: a whole 2x2x4 slice. The times are simulated.
32 devices in a mesh: ep: 32 (over z, y, x, core).
Axes of the slice: x: 2, y: 2, z: 4, core: 2. Of those that a mesh axis runs over, the one named last changes fastest.
Arguments:
- tokens: bfloat16 [512, 2048], P('ep'), may hold values from -6 to 6
- hidden_state: float32 [512, 1024], P('ep'), may hold values from -3 to 3
- recent_inputs: bfloat16 [512, 3, 1024], P('ep'), may hold values from -6 to 6
- routes: int32 [512, 2], P('ep'), may hold values from 0 to 7, all different within a row; in each aligned block of 16 rows (0 to 15, 16 to 31, ...) at most 8 rows name the same one
- gain_mix: bfloat16 [2048], replicated, may hold values from 0.099609375 to 1.8984375
- input_weight: bfloat16 [2048, 1024], replicated, may hold values from -0.125 to 0.125
- branch_weight: bfloat16 [2048, 1024], replicated, may hold values from -0.125 to 0.125
- filter_taps: bfloat16 [4, 1024], replicated, may hold values from -3 to 3
- recurrence_map: bfloat16 [8, 128, 128], replicated, may hold values from -0.5 to 0.5
- input_map: bfloat16 [8, 128, 128], replicated, may hold values from -0.5 to 0.5
- decay_param: float32 [1024], replicated, may hold values from 0.5 to 6
- output_weight: bfloat16 [1024, 2048], replicated, may hold values from -0.1875 to 0.1875
- gain_experts: bfloat16 [2048], replicated, may hold values from 0.099609375 to 1.8984375
- router_weight: bfloat16 [2048, 8], replicated, may hold values from -0.125 to 0.125
- expert_gate: bfloat16 [2048, 32768], P(None, 'ep'), may hold values from -0.125 to 0.125
- expert_up: bfloat16 [2048, 32768], P(None, 'ep'), may hold values from -0.125 to 0.125
- expert_down: bfloat16 [32768, 2048], P('ep'), may hold values from -0.09375 to 0.09375
Outputs:
- layer_out: bfloat16 [512, 2048], P('ep')
- new_hidden: float32 [512, 1024], P('ep')
- new_inputs: bfloat16 [512, 3, 1024], P('ep')
Inputs may be any that keep to these rules, and one draw needn't show every extreme that they name: `routes`: each row names 2 different experts. The rows of one device name one expert at most 8 times; in every draw some device names some expert exactly 8 times.
All inputs are finite; a program needn't handle non-finite values.
Results may differ from a plain program's by a relative error of at most 0.01.
Values may be sent and summed in bfloat16 or wider, within the bound.
A program may use at most 128 MiB of HBM per device.

v0:
```python
import jax
import jax.numpy as jnp
from jax import lax
from jax.sharding import PartitionSpec as P

EXPERTS = 8
CAP = 8


epsilon = 1e-06
rate_scale = 8.0


def rms_scale(values, gain):
    mean_square = jnp.mean(values * values, axis=-1, keepdims=True)
    return values * lax.rsqrt(mean_square + epsilon) * gain.astype(jnp.float32)


def mixer_step(
    tokens,
    hidden_state,
    recent_inputs,
    gain_mix,
    input_weight,
    branch_weight,
    filter_taps,
    recurrence_map,
    input_map,
    decay_param,
    output_weight,
):
    resid = tokens.astype(jnp.float32)
    normed = rms_scale(resid, gain_mix).astype(jnp.bfloat16)
    branch_x = jnp.dot(normed, input_weight, preferred_element_type=jnp.float32).astype(
        jnp.bfloat16
    )
    branch_g = jnp.dot(normed, branch_weight, preferred_element_type=jnp.float32).astype(
        jnp.bfloat16
    )
    window = jnp.concatenate([recent_inputs, branch_x[:, None, :]], axis=1)
    new_inputs = window[:, 1:, :]
    conv_out = jnp.sum(
        window.astype(jnp.float32) * filter_taps.astype(jnp.float32)[None], axis=1
    ).astype(jnp.bfloat16)
    width = recurrence_map.shape[1]
    blocks = conv_out.reshape(conv_out.shape[0], -1, width)
    rec_gate = jax.nn.sigmoid(
        jnp.einsum(
            "sni,nij->snj", blocks, recurrence_map, preferred_element_type=jnp.float32
        ).reshape(conv_out.shape)
    )
    in_gate = jax.nn.sigmoid(
        jnp.einsum("sni,nij->snj", blocks, input_map, preferred_element_type=jnp.float32).reshape(
            conv_out.shape
        )
    )
    log_decay = -rate_scale * rec_gate * jax.nn.softplus(-decay_param)
    new_hidden = jnp.exp(log_decay) * hidden_state + jnp.sqrt(-jnp.expm1(2.0 * log_decay)) * (
        in_gate * conv_out.astype(jnp.float32)
    )
    mixed = (new_hidden * jax.nn.gelu(branch_g.astype(jnp.float32))).astype(jnp.bfloat16)
    after = resid + jnp.dot(mixed, output_weight, preferred_element_type=jnp.float32)
    return (after, new_hidden, new_inputs)


def route_weights(normed_rows, router_weight, routes):
    logits = jnp.dot(normed_rows, router_weight, preferred_element_type=jnp.float32)
    expert_ids = jnp.arange(router_weight.shape[1], dtype=jnp.int32)
    picks = routes[:, :, None] == expert_ids[None, None, :]
    chosen = jnp.sum(jnp.where(picks, logits[:, None, :], jnp.float32(0.0)), axis=-1)
    spread = chosen[:, 0] - chosen[:, 1]
    share = jnp.stack([jax.nn.sigmoid(spread), jax.nn.sigmoid(-spread)], axis=1)
    return jnp.sum(jnp.where(picks, share[:, :, None], jnp.float32(0.0)), axis=1)


def slot_table(route_blocks, expert_ids, capacity):
    member = jnp.any(route_blocks[:, :, :, None] == expert_ids[None, None, None, :], axis=2)
    order = jnp.cumsum(member.astype(jnp.int32), axis=1) - 1
    slot_ids = jnp.arange(capacity, dtype=jnp.int32)
    return (member[..., None] & (order[..., None] == slot_ids)).astype(jnp.float32)


def expert_rows(packed, gate_cols, up_cols, down_rows):
    gate = jnp.dot(packed, gate_cols, preferred_element_type=jnp.float32)
    upper = jnp.dot(packed, up_cols, preferred_element_type=jnp.float32)
    inner = (jax.nn.silu(gate) * upper).astype(jnp.bfloat16)
    return jnp.dot(inner, down_rows, preferred_element_type=jnp.float32)


def local(
    tokens,
    hidden_state,
    recent_inputs,
    routes,
    gain_mix,
    input_weight,
    branch_weight,
    filter_taps,
    recurrence_map,
    input_map,
    decay_param,
    output_weight,
    gain_experts,
    router_weight,
    expert_gate,
    expert_up,
    expert_down,
):
    after, new_hidden, new_inputs = mixer_step(
        tokens,
        hidden_state,
        recent_inputs,
        gain_mix,
        input_weight,
        branch_weight,
        filter_taps,
        recurrence_map,
        input_map,
        decay_param,
        output_weight,
    )
    expert_in = rms_scale(after, gain_experts).astype(jnp.bfloat16)
    devices = lax.axis_size("ep")
    group = devices // EXPERTS
    width = expert_in.shape[1]
    weight_table = route_weights(expert_in, router_weight, routes)
    all_ids = jnp.arange(EXPERTS, dtype=jnp.int32)
    table = slot_table(routes[None], all_ids, CAP)[0]
    packed = jnp.einsum(
        "sec,sd->ecd", table.astype(jnp.bfloat16), expert_in, preferred_element_type=jnp.float32
    ).astype(jnp.bfloat16)
    outgoing = jnp.repeat(packed, group, axis=0)
    arrived = lax.all_to_all(outgoing, "ep", split_axis=0, concat_axis=0, tiled=True)
    partial_out = expert_rows(arrived.reshape(-1, width), expert_gate, expert_up, expert_down)
    partial_out = partial_out.reshape(arrived.shape)
    returned = lax.all_to_all(partial_out, "ep", split_axis=0, concat_axis=0, tiled=True)
    results = jnp.sum(returned.reshape(EXPERTS, group, CAP, width), axis=1)
    scaled = table * weight_table[:, :, None]
    total = jnp.einsum("sec,ecd->sd", scaled, results, precision=lax.Precision.HIGHEST)
    layer_out = (after + total).astype(jnp.bfloat16)
    return (layer_out, new_hidden, new_inputs)


def solution(mesh):
    placed = (
        P("ep", None),
        P("ep", None),
        P("ep", None, None),
        P("ep", None),
        P(),
        P(),
        P(),
        P(),
        P(),
        P(),
        P(),
        P(),
        P(),
        P(),
        P(None, "ep"),
        P(None, "ep"),
        P("ep", None),
    )
    return jax.shard_map(
        local,
        mesh=mesh,
        in_specs=placed,
        out_specs=(P("ep", None), P("ep", None), P("ep", None, None)),
        check_vma=False,
    )
```

profile of v0, /device:TPU:0, one launch (start us, length us, event | category | flops | bytes accessed | tf_op | source)
XLA Modules:
  0.0 110.1 jit_solution(14121738532418157071)
XLA Ops:
  0.6 0.0 copy-start
  0.6 0.0 copy-start.1
  0.7 0.0 copy-start.2
  0.7 0.0 copy-start.9
  0.7 0.0 copy-start.8
  0.7 0.0 copy-start.4
  0.7 0.8 convert_element_type.73
  1.4 1.0 fusion.20
  2.4 0.7 convert_element_type.77
  3.1 2.9 %fusion.12 = bf16[16,1,1024]{2,0,1:T(8,128)(2,1)S(1)} fusion(bf16[2048,1024]{1,0:T(8,128)(2,1)} %param.22, bf16[16,2048]{1,0:T(8,128)(2,1)} %param.17, f32[2048]{0:T(1024)S(1)} %convert_element_type.73, f32[16]{0:T(128)S(1)} %add_rsqrt_fusion.1), kind=kOutput, calls=%fused_computation.22 | convolution fusion | flops 67256320 | bytes 4300864 | tf_op jit(solution)/shard_map/dot_general | solution.py:34
  6.1 0.0 copy-done.2
  6.1 0.0 copy-done
  6.1 0.2 fusion.10
  6.3 0.0 copy-done.9
  6.3 0.2 fusion.6
  6.5 0.0 copy-done.8
  6.5 0.0 copy-done.4
  6.5 0.1 fusion.34
  6.6 0.0 copy-done.1
  6.6 0.0 copy-start.3
  6.6 0.0 copy-start.6
  6.7 0.0 copy-start.7
  6.7 4.9 %multiply_reduce_fusion.1 = (f32[16]{0:T(128)S(1)}, f32[16,2048]{1,0:T(8,128)S(1)}) fusion(bf16[1024,2048]{1,0:T(8,128)(2,1)} %param.28, f32[16,1024]{1,0:T(8,128)S(1)} %fusion.34, bf16[2048,1024]{1,0:T(8,128)(2,1)} %param.23, bf16[16,2048]{1,0:T(8,128)(2,1)S(1)} %copy-done.1, f32[2048]{0:T(1024)S(1)} %convert_element_type.73, f32[16]{0:T(128)S(1)} %add_rsqrt_fusion.1), kind=kOutput, calls=%fused_computation.38 | convolution fusion | flops 134676464 | bytes 8659072 | tf_op jit(solution)/shard_map/dot_general | solution.py:62
  11.5 0.0 copy-done.3
  11.6 0.0 copy-done.6
  11.6 0.1 copy.54
  11.7 0.1 copy.55
  11.8 0.0 copy-done.7
  11.8 0.3 convolution_convert_fusion
  12.1 0.1 broadcast_in_dim.30
  12.2 33.3 %all_to_all.10 = bf16[32,8,2048]{2,1,0:T(8,128)(2,1)S(1)} all-to-all(bf16[32,8,2048]{2,1,0:T(8,128)(2,1)S(1)} %bitcast.62), channel_id=1, replica_groups=mesh['ep'=32] {'ep'}, dimensions={0} | all-to-all | bytes 2097152 | tf_op jit(solution)/shard_map/all_to_all | solution.py:133
  45.6 3.5 %fusion.14 = f32[256,1024]{1,0:T(8,128)S(1)} fusion(bf16[2048,1024]{1,0:T(8,128)(2,1)} %param.31, bf16[32,8,2048]{2,1,0:T(8,128)(2,1)S(1)} %all_to_all.10), kind=kOutput, calls=%fused_computation.24 | convolution fusion | flops 1073741824 | bytes 6291456 | tf_op jit(solution)/shard_map/dot_general | solution.py:84
  49.0 7.4 %convolution_bitcast_fusion = f32[32,8,2048]{2,1,0:T(8,128)} fusion(bf16[1024,2048]{1,0:T(8,128)(2,1)} %param.33, bf16[2048,1024]{1,0:T(8,128)(2,1)} %param.32, bf16[32,8,2048]{2,1,0:T(8,128)(2,1)S(1)} %all_to_all.10, f32[256,1024]{1,0:T(8,128)S(1)} %fusion.14), kind=kOutput, calls=%fused_computation | convolution fusion | flops 2149056512 | bytes 12582912 | tf_op jit(solution)/shard_map/dot_general | solution.py:87
  56.4 0.0 copy-start.5
  56.4 3.6 %all-to-all-start.1 = ((f32[32,8,2048]{2,1,0:T(8,128)}), f32[32,8,2048]{2,1,0:T(8,128)S(1)}, u32[]{:S(2)}, u32[]{:S(2)}) async-start(f32[32,8,2048]{2,1,0:T(8,128)} %convolution_bitcast_fusion), calls=%async_computation.1 | async-start | bytes 4194304 | tf_op jit(solution)/shard_map/all_to_all | solution.py:136
  60.0 0.0 copy-done.5
  60.0 0.2 fusion.66
  60.3 0.7 fusion.23
  61.0 47.8 %all-to-all-done.1 = f32[32,8,2048]{2,1,0:T(8,128)S(1)} async-done(((f32[32,8,2048]{2,1,0:T(8,128)}), f32[32,8,2048]{2,1,0:T(8,128)S(1)}, u32[]{:S(2)}, u32[]{:S(2)}) %all-to-all-start.1) | async-done | bytes 2097184 | tf_op jit(solution)/shard_map/all_to_all | solution.py:136
  108.8 0.1 bitcast_reduce_fusion
  108.9 1.3 %fusion.1 = bf16[16,2048]{1,0:T(8,128)(2,1)} fusion(f32[16,2048]{1,0:T(8,128)S(1)} %get-tuple-element.6, f32[8,8,2048]{2,1,0:T(8,128)S(1)} %bitcast_reduce_fusion, f32[16,8]{0,1:T(8,128)S(1)} %select_reduce_fusion, s32[16,8]{0,1:T(8,128)S(1)} %copy.55, pred[16,8]{0,1:T(8,128)(4,1)S(1)} %fusion.58), kind=kOutput, calls=%fused_computation.5 | convolution fusion | flops 25234432 | bytes 722048 | tf_op jit(solution)/shard_map/sec,ecd->sd/dot_general | solution.py:139
  (14 shorter events, 0.2 us)
Async XLA Ops:
  0.6 5.5 %copy-start = (bf16[8,128,128]{2,1,0:T(8,128)(2,1)S(1)}, bf16[8,128,128]{2,1,0:T(8,128)(2,1)}, u32[]{:S(2)}) copy-start(bf16[8,128,128]{2,1,0:T(8,128)(2,1)} %param.25) | copy-start | bytes 786436
  0.6 6.0 %copy-start.1 = (bf16[16,2048]{1,0:T(8,128)(2,1)S(1)}, bf16[16,2048]{1,0:T(8,128)(2,1)}, u32[]{:S(2)}) copy-start(bf16[16,2048]{1,0:T(8,128)(2,1)} %param.17) | copy-start | bytes 196612
  0.7 5.4 %copy-start.2 = (bf16[16,3,1024]{2,0,1:T(8,128)(2,1)S(1)}, bf16[16,3,1024]{2,0,1:T(8,128)(2,1)}, u32[]{:S(2)}) copy-start(bf16[16,3,1024]{2,0,1:T(8,128)(2,1)} %param.19) | copy-start | bytes 294916
  0.7 5.6 %copy-start.9 = (bf16[8,128,128]{2,1,0:T(8,128)(2,1)S(1)}, bf16[8,128,128]{2,1,0:T(8,128)(2,1)}, u32[]{:S(2)}) copy-start(bf16[8,128,128]{2,1,0:T(8,128)(2,1)} %param.26) | copy-start | bytes 786436
  0.7 5.8 %copy-start.8 = (f32[1024]{0:T(1024)S(1)}, f32[1024]{0:T(1024)}, u32[]{:S(2)}) copy-start(f32[1024]{0:T(1024)} %param.27) | copy-start | bytes 12292
  0.7 5.9 %copy-start.4 = (f32[16,1024]{1,0:T(8,128)S(1)}, f32[16,1024]{1,0:T(8,128)}, u32[]{:S(2)}) copy-start(f32[16,1024]{1,0:T(8,128)} %param.18) | copy-start | bytes 196612
  6.6 4.9 %copy-start.3 = (f32[16,1024]{1,0:T(8,128)}, f32[16,1024]{1,0:T(8,128)S(1)}, u32[]{:S(2)}) copy-start(f32[16,1024]{1,0:T(8,128)S(1)} %fusion.34) | copy-start | bytes 196612
  6.6 4.9 %copy-start.6 = (s32[16,2]{0,1:T(2,128)S(1)}, s32[16,2]{0,1:T(2,128)}, u32[]{:S(2)}) copy-start(s32[16,2]{0,1:T(2,128)} %param.20) | copy-start | bytes 388
  6.7 5.2 %copy-start.7 = (bf16[2048]{0:T(1024)(128)(2,1)S(1)}, bf16[2048]{0:T(1024)(128)(2,1)}, u32[]{:S(2)}) copy-start(bf16[2048]{0:T(1024)(128)(2,1)} %param.29) | copy-start | bytes 12292
  56.4 3.6 %copy-start.5 = (bf16[2048,8]{0,1:T(8,128)(2,1)S(1)}, bf16[2048,8]{0,1:T(8,128)(2,1)}, u32[]{:S(2)}) copy-start(bf16[2048,8]{0,1:T(8,128)(2,1)} %param.30) | copy-start | bytes 98308
  56.4 52.4 %all-to-all-start.1 = ((f32[32,8,2048]{2,1,0:T(8,128)}), f32[32,8,2048]{2,1,0:T(8,128)S(1)}, u32[]{:S(2)}, u32[]{:S(2)}) async-start(f32[32,8,2048]{2,1,0:T(8,128)} %convolution_bitcast_fusion), calls=%async_computation.1 | async-start | bytes 4194304 | tf_op jit(solution)/shard_map/all_to_all | solution.py:136
where the time goes:
time: 111 us; the launch traced here: 110 us
  waiting for transfers between devices  47.8 us (43%)
  blocking collectives  33.3 us (30%)
  matrix products  20.7 us (19%)
  starting transfers between devices  3.62 us (3%)
  other arithmetic  3.44 us (3%)
    all_to_all x1, waiting for transfers between devices, local(): lax.all_to_all(partial_out, 'ep', split_axis=0, concat_axis=0, tiled=True)  47.8 us
    all_to_all x1, blocking collectives, local(): lax.all_to_all(outgoing, 'ep', split_axis=0, concat_axis=0, tiled=True)  33.3 us
    dot_general x1, matrix products, expert_rows(): return jnp.dot(inner, down_rows, preferred_element_type=jnp.float32)  7.38 us
    dot_general x1, matrix products, mixer_step(): jnp.dot(mixed, output_weight, preferred_element_type=jnp.float32)  4.87 us
    all_to_all x1, starting transfers between devices, local(): lax.all_to_all(partial_out, 'ep', split_axis=0, concat_axis=0, tiled=True)  3.62 us
    dot_general x1, matrix products, expert_rows(): gate = jnp.dot(packed, gate_cols, preferred_element_type=jnp.float32)  3.45 us
    dot_general x1, matrix products, mixer_step(): jnp.dot(normed, input_weight, preferred_element_type=jnp.float32)  2.92 us
  transfers between devices with their start and end apart: 1, of which 1 were waited for; matrix products, arithmetic and copies ran while one was open for 1% of the time, Pallas kernels for 0%

commit v1 on v0

v1 whole, which is shorter than its diff:
```python
import functools

import jax
import jax.numpy as jnp
from jax import lax
from jax.experimental import pallas as pl
from jax.experimental.pallas import tpu as pltpu
from jax.sharding import PartitionSpec as P

EXPERTS = 8
CAP = 8
TAPS = 4
BITS = 3
ORDER = (1, 4, 6, 2, 5, 7, 3)

epsilon = 1e-06
rate_scale = 8.0

f32 = jnp.float32
bf16 = jnp.bfloat16


def rms_scale(values, gain):
    mean_square = jnp.mean(values * values, axis=-1, keepdims=True)
    return values * lax.rsqrt(mean_square + epsilon) * gain.astype(f32)


def flip(e, k):
    out = 0
    for i in range(BITS):
        bit = (e // (1 << i)) % 2
        if (k >> i) & 1:
            bit = 1 - bit
        out = out + bit * (1 << i)
    return out


def kernel(
    n,
    n_col,
    tokens,
    hidden_state,
    recent,
    routes,
    gain_mix,
    filter_taps,
    recurrence_map,
    input_map,
    decay_param,
    gain_experts,
    router_weight,
    w_in_hbm,
    w_branch_hbm,
    w_out_hbm,
    w_gate_hbm,
    w_up_hbm,
    w_down_hbm,
    layer_out,
    new_hidden_out,
    branch_out,
    w_in,
    w_branch,
    w_out,
    w_gate,
    w_up,
    w_down,
    after_ref,
    packed,
    x_blocks,
    x_rows,
    inner,
    a_send,
    a_recv,
    keep,
    b_send,
    b_recv,
    keep_own,
    c_send,
    c_recv,
    w_sem,
    d1_s,
    d1_r,
    d2_s,
    d2_r,
    d3_s,
    d3_r,
    a_s,
    a_r,
    b_s,
    b_r,
    c_s,
    c_r,
):
    me = lax.axis_index("ep")
    group = n // EXPERTS
    chips = group // 2
    e = me // group
    q = me % group
    core = me % 2
    chip = q // 2
    partner = me + 1 - 2 * core

    def peer_chip(d):
        return e * group + ((chip + d) % chips) * 2 + core

    def remote(src, dst, ssem, rsem, dev):
        return pltpu.make_async_remote_copy(
            src_ref=src,
            dst_ref=dst,
            send_sem=ssem,
            recv_sem=rsem,
            device_id=(dev,),
            device_id_type=pl.DeviceIdType.MESH,
        )

    barrier = pltpu.get_barrier_semaphore()
    peers = [flip(e, k) * group + q for k in range(1, EXPERTS)]
    peers += [partner] + [peer_chip(d) for d in range(1, chips)]
    for dev in peers:
        pl.semaphore_signal(
            barrier, inc=1, device_id=(dev,), device_id_type=pl.DeviceIdType.MESH
        )

    parts = 4
    loads = []

    def load(src, dst, pieces):
        rows = src.shape[0] // pieces
        made = []
        for i in range(pieces):
            cut = pl.ds(i * rows, rows)
            made.append(pltpu.make_async_copy(src.at[cut], dst.at[cut], w_sem.at[len(loads)]))
            loads.append(made[-1])
        return made

    in_loads = load(w_in_hbm, w_in, parts)
    branch_loads = load(w_branch_hbm, w_branch, parts)
    out_loads = load(w_out_hbm, w_out, parts)
    expert_loads = load(w_gate_hbm, w_gate, 1) + load(w_up_hbm, w_up, 1) + load(w_down_hbm, w_down, 1)
    for copy in loads:
        copy.start()

    def streamed(lhs, weight, copies):
        rows = weight.shape[0] // len(copies)
        total = None
        for i, copy in enumerate(copies):
            copy.wait()
            part = jnp.dot(
                lhs[:, i * rows : (i + 1) * rows],
                weight[i * rows : (i + 1) * rows, :],
                preferred_element_type=f32,
            )
            total = part if total is None else total + part
        return total

    resid = tokens[...].astype(f32)
    normed = rms_scale(resid, gain_mix[...]).astype(bf16)
    branch_x = streamed(normed, w_in, in_loads).astype(bf16)
    branch_out[...] = branch_x
    rnn = branch_x.shape[1]
    taps = filter_taps[...].astype(f32)
    conv = branch_x.astype(f32) * taps[TAPS - 1 : TAPS]
    for j in range(TAPS - 1):
        conv = conv + recent[:, j * rnn : (j + 1) * rnn].astype(f32) * taps[j : j + 1]
    conv_out = conv.astype(bf16)
    width = recurrence_map.shape[1]
    blocks = rnn // width
    rec = jnp.concatenate(
        [
            jnp.dot(conv_out[:, i * width : (i + 1) * width], recurrence_map[i], preferred_element_type=f32)
            for i in range(blocks)
        ],
        axis=1,
    )
    ing = jnp.concatenate(
        [
            jnp.dot(conv_out[:, i * width : (i + 1) * width], input_map[i], preferred_element_type=f32)
            for i in range(blocks)
        ],
        axis=1,
    )
    rec_gate = jax.nn.sigmoid(rec)
    in_gate = jax.nn.sigmoid(ing)
    neg = -decay_param[...]
    soft = jnp.maximum(neg, 0.0) + jnp.log1p(jnp.exp(-jnp.abs(neg)))
    log_decay = -rate_scale * rec_gate * soft
    decay = jnp.exp(log_decay)
    lost = -jnp.tanh(log_decay) * (decay * decay + 1.0)
    new_hidden = decay * hidden_state[...] + jnp.sqrt(lost) * (in_gate * conv_out.astype(f32))
    new_hidden_out[...] = new_hidden
    branch_g = streamed(normed, w_branch, branch_loads).astype(bf16).astype(f32)
    mixed = (new_hidden * jax.nn.gelu(branch_g, approximate=True)).astype(bf16)
    after = resid + streamed(mixed, w_out, out_loads)
    after_ref[...] = after
    expert_in = rms_scale(after, gain_experts[...]).astype(bf16)

    seq = expert_in.shape[0]
    slots = EXPERTS * CAP
    col = lax.broadcasted_iota(jnp.int32, (seq, slots), 1)
    first = routes[:, 0:1]
    second = routes[:, 1:2]
    pick0 = (col // CAP) == first
    pick1 = (col // CAP) == second
    member = (pick0 | pick1).astype(f32)
    tri = (
        lax.broadcasted_iota(jnp.int32, (seq, seq), 0) >= lax.broadcasted_iota(jnp.int32, (seq, seq), 1)
    ).astype(f32)
    rank = jnp.dot(tri.astype(bf16), member.astype(bf16), preferred_element_type=f32)
    table = jnp.where(rank == (col % CAP + 1).astype(f32), member, 0.0)

    dense = lax.dot_general(
        table.astype(bf16), expert_in, (((0,), (0,)), ((), ())), preferred_element_type=f32
    )
    packed[...] = dense.reshape(packed.shape).astype(bf16)

    pl.semaphore_wait(barrier, len(peers))

    sends = []
    for k in ORDER:
        f = flip(e, k)
        copy = remote(packed.at[f], x_blocks.at[0, 0, e], d1_s.at[k], d1_r.at[k], f * group + q)
        copy.start()
        sends.append(copy)
    x_blocks[0, 0, e] = packed[e]

    logits = jnp.dot(expert_in, router_weight[...], preferred_element_type=f32)
    ids = lax.broadcasted_iota(jnp.int32, logits.shape, 1)
    l0 = jnp.sum(jnp.where(ids == first, logits, 0.0), axis=1, keepdims=True)
    l1 = jnp.sum(jnp.where(ids == second, logits, 0.0), axis=1, keepdims=True)
    share0 = jax.nn.sigmoid(l0 - l1)
    share1 = jax.nn.sigmoid(l1 - l0)
    scaled = table * (jnp.where(pick0, share0, 0.0) + jnp.where(pick1, share1, 0.0))
    high = scaled.astype(bf16)
    low = (scaled - high.astype(f32)).astype(bf16)
    combine = jnp.concatenate([high, low], axis=0)

    def spread(k):
        f = flip(e, k)
        for d in range(1, chips):
            copy = remote(
                x_blocks.at[0, 0, f],
                x_blocks.at[0, chips - d, f],
                d2_s.at[d - 1, k],
                d2_r.at[chips - d - 1, k],
                peer_chip(d),
            )
            copy.start()
            sends.append(copy)
        copy = remote(x_blocks.at[0, 0, f], x_blocks.at[1, 0, f], d3_s.at[0, k], d3_r.at[0, k], partner)
        copy.start()
        sends.append(copy)

    def arrived(buf, ssem, rsem):
        remote(buf, buf, ssem, rsem, partner).wait_recv()

    spread(0)
    for k in ORDER:
        arrived(x_blocks.at[0, 0, flip(e, k)], d1_s.at[k], d1_r.at[k])
        spread(k)

    block_rows = EXPERTS * CAP
    model = x_rows.shape[1]

    def flatten(c, d):
        at = (c * chips + d) * block_rows
        x_rows[at : at + block_rows, :] = (
            x_blocks[c, d].astype(f32).reshape(block_rows, model).astype(bf16)
        )

    for k in (0,) + ORDER:
        for d in range(1, chips):
            f = flip(e, k)
            arrived(x_blocks.at[0, d, f], d2_s.at[d - 1, k], d2_r.at[d - 1, k])
            copy = remote(x_blocks.at[0, d, f], x_blocks.at[1, d, f], d3_s.at[d, k], d3_r.at[d, k], partner)
            copy.start()
            sends.append(copy)
    for d in range(chips):
        flatten(0, d)
    for d in range(chips):
        for k in (0,) + ORDER:
            arrived(x_blocks.at[1, d, flip(e, k)], d3_s.at[d, k], d3_r.at[d, k])
        flatten(1, d)

    for copy in expert_loads:
        copy.wait()
    hidden = w_gate.shape[1]
    step = min(256, hidden)

    def hidden_chunk(j, carry):
        cut = pl.ds(pl.multiple_of(j * step, step), step)
        rows = x_rows[...]
        gate = jnp.dot(rows, w_gate[:, cut], preferred_element_type=f32)
        upper = jnp.dot(rows, w_up[:, cut], preferred_element_type=f32)
        inner[:, cut] = (gate * jax.nn.sigmoid(gate) * upper).astype(bf16)
        return carry

    lax.fori_loop(0, hidden // step, hidden_chunk, 0)

    half = chips * block_rows
    wide = model // n_col

    def down(c):
        out = jnp.dot(inner[...], w_down[:, c * wide : (c + 1) * wide], preferred_element_type=f32)
        a_send[c] = out[half:, :].astype(bf16)
        keep[c] = out[:half, :]
        copy = remote(a_send.at[c], a_recv.at[c], a_s.at[c], a_r.at[c], partner)
        copy.start()
        sends.append(copy)

    def across(c):
        arrived(a_recv.at[c], a_s.at[c], a_r.at[c])
        both = keep[c] + a_recv[c].astype(f32)
        for d in range(1, chips):
            b_send[d - 1, c] = both[d * block_rows : (d + 1) * block_rows, :].astype(bf16)
            copy = remote(
                b_send.at[d - 1, c],
                b_recv.at[chips - d - 1, c],
                b_s.at[d - 1, c],
                b_r.at[chips - d - 1, c],
                peer_chip(d),
            )
            copy.start()
            sends.append(copy)
        keep_own[c] = both[:block_rows, :]

    def home(c):
        total = keep_own[c]
        for d in range(1, chips):
            arrived(b_recv.at[d - 1, c], b_s.at[d - 1, c], b_r.at[d - 1, c])
            total = total + b_recv[d - 1, c].astype(f32)
        c_send[c] = total.reshape(EXPERTS, CAP, wide).astype(bf16)
        for k in ORDER:
            f = flip(e, k)
            copy = remote(c_send.at[c, f], c_recv.at[c, e], c_s.at[k, c], c_r.at[k, c], f * group + q)
            copy.start()
            sends.append(copy)
        c_recv[c, e] = c_send[c, e]

    def finish(c):
        for k in ORDER:
            arrived(c_recv.at[c, flip(e, k)], c_s.at[k, c], c_r.at[k, c])
        results = c_recv[c].astype(f32).reshape(slots, wide).astype(bf16)
        both = jnp.dot(combine, results, preferred_element_type=f32)
        cut = slice(c * wide, (c + 1) * wide)
        layer_out[:, cut] = (after_ref[:, cut] + (both[:seq] + both[seq:])).astype(bf16)

    for c in range(n_col):
        down(c)
        if c:
            across(c - 1)
    across(n_col - 1)
    for c in range(n_col):
        home(c)
    for c in range(n_col):
        finish(c)
    for copy in sends:
        copy.wait_send()


def solution(mesh):
    n = mesh.shape["ep"]

    def local(
        tokens,
        hidden_state,
        recent_inputs,
        routes,
        gain_mix,
        input_weight,
        branch_weight,
        filter_taps,
        recurrence_map,
        input_map,
        decay_param,
        output_weight,
        gain_experts,
        router_weight,
        expert_gate,
        expert_up,
        expert_down,
    ):
        seq, model = tokens.shape
        rnn = hidden_state.shape[1]
        hidden = expert_gate.shape[1]
        group = n // EXPERTS
        chips = group // 2
        rows = n * CAP
        block = EXPERTS * CAP
        n_col = 4
        wide = model // n_col
        dma = pltpu.SemaphoreType.DMA
        vmem = pl.BlockSpec(memory_space=pltpu.VMEM)
        hbm = pl.BlockSpec(memory_space=pl.ANY)
        far = max(chips - 1, 1)
        layer_out, new_hidden, branch_x = pl.pallas_call(
            functools.partial(kernel, n, n_col),
            out_shape=(
                jax.ShapeDtypeStruct((seq, model), bf16),
                jax.ShapeDtypeStruct((seq, rnn), f32),
                jax.ShapeDtypeStruct((seq, rnn), bf16),
            ),
            in_specs=[vmem] * 11 + [hbm] * 6,
            out_specs=(vmem, vmem, vmem),
            scratch_shapes=[
                pltpu.VMEM(input_weight.shape, bf16),
                pltpu.VMEM(branch_weight.shape, bf16),
                pltpu.VMEM(output_weight.shape, bf16),
                pltpu.VMEM(expert_gate.shape, bf16),
                pltpu.VMEM(expert_up.shape, bf16),
                pltpu.VMEM(expert_down.shape, bf16),
                pltpu.VMEM((seq, model), f32),
                pltpu.VMEM((EXPERTS, CAP, model), bf16),
                pltpu.VMEM((2, chips, EXPERTS, CAP, model), bf16),
                pltpu.VMEM((rows, model), bf16),
                pltpu.VMEM((rows, hidden), bf16),
                pltpu.VMEM((n_col, rows // 2, wide), bf16),
                pltpu.VMEM((n_col, rows // 2, wide), bf16),
                pltpu.VMEM((n_col, rows // 2, wide), f32),
                pltpu.VMEM((far, n_col, block, wide), bf16),
                pltpu.VMEM((far, n_col, block, wide), bf16),
                pltpu.VMEM((n_col, block, wide), f32),
                pltpu.VMEM((n_col, EXPERTS, CAP, wide), bf16),
                pltpu.VMEM((n_col, EXPERTS, CAP, wide), bf16),
                dma((16,)),
                dma((EXPERTS,)),
                dma((EXPERTS,)),
                dma((far, EXPERTS)),
                dma((far, EXPERTS)),
                dma((chips, EXPERTS)),
                dma((chips, EXPERTS)),
                dma((n_col,)),
                dma((n_col,)),
                dma((far, n_col)),
                dma((far, n_col)),
                dma((EXPERTS, n_col)),
                dma((EXPERTS, n_col)),
            ],
            compiler_params=pltpu.CompilerParams(
                collective_id=0, has_side_effects=True, vmem_limit_bytes=60 * 1024 * 1024
            ),
        )(
            tokens,
            hidden_state,
            recent_inputs.reshape(seq, -1),
            routes,
            gain_mix[None],
            filter_taps,
            recurrence_map,
            input_map,
            decay_param[None],
            gain_experts[None],
            router_weight,
            input_weight,
            branch_weight,
            output_weight,
            expert_gate,
            expert_up,
            expert_down,
        )
        new_inputs = jnp.concatenate([recent_inputs[:, 1:, :], branch_x[:, None, :]], axis=1)
        return (layer_out, new_hidden, new_inputs)

    placed = (
        P("ep", None),
        P("ep", None),
        P("ep", None, None),
        P("ep", None),
    ) + (P(),) * 10 + (P(None, "ep"), P(None, "ep"), P("ep", None))
    return jax.shard_map(
        local,
        mesh=mesh,
        in_specs=placed,
        out_specs=(P("ep", None), P("ep", None), P("ep", None, None)),
        check_vma=False,
    )
```

time: 111 us -> 52.1 us (0.47)
  waiting for transfers between devices: 47.8 us -> 0 us
  Pallas kernels: 0 us -> 39.4 us
  blocking collectives: 33.3 us -> 0 us
  matrix products: 20.7 us -> 0 us
  local copies, waits for them, and re-layouts: 0.31 us -> 10.2 us
  starting transfers between devices: 3.62 us -> 0 us
  other arithmetic: 3.44 us -> 1.41 us
    all_to_all x1 -> x0, waiting for transfers between devices: 47.8 us -> none  [local(): lax.all_to_all(partial_out, 'ep', split_axis=0, concat_axis=0, tiled=True)]
    pallas_call x0 -> x1, Pallas kernels: none -> 39.4 us  [local(): pl.pallas_call(functools.partial(kernel, n, n_col), out_shape=(jax.ShapeD...]
    all_to_all x1 -> x0, blocking collectives: 33.3 us -> none  [local(): lax.all_to_all(outgoing, 'ep', split_axis=0, concat_axis=0, tiled=True)]
    dot_general x9 -> x0, matrix products: 20.7 us -> none  [the longest x1 7.38 us: expert_rows(): return jnp.dot(inner, down_rows, preferred_element_type=jnp.float32)]
    unnamed x20 -> x6, local copies, waits for them, and re-layouts: 0.06 us -> 6.05 us
    all_to_all x1 -> x0, starting transfers between devices: 3.62 us -> none  [local(): lax.all_to_all(partial_out, 'ep', split_axis=0, concat_axis=0, tiled=True)]
    broadcast_in_dim x1 -> x2, local copies, waits for them, and re-layouts: 0.11 us -> 2.57 us  [the longest x1 1.29 us: local(): gain_mix[None]]
    reshape x0 -> x1, local copies, waits for them, and re-layouts: none -> 1.54 us  [local(): recent_inputs.reshape(seq, -1)]
  transfers between devices with their start and end apart: 1 -> 0, of which waited for: 1 -> 0; matrix products, arithmetic and copies ran while one was open for 1% -> 0% of each run, Pallas kernels for 0% -> 0%
where the time goes in v1:
time: 52.1 us; the launch traced here: 51.7 us
  Pallas kernels  39.4 us (76%)
  local copies, waits for them, and re-layouts  10.2 us (20%)
  other arithmetic  1.41 us (3%)
  between operations  0.66 us (1%)
    pallas_call x1, Pallas kernels, local(): pl.pallas_call(functools.partial(kernel, n, n_col), out_shape=(jax.ShapeD...  39.4 us
    unnamed x6, local copies, waits for them, and re-layouts  6.05 us
    reshape x1, local copies, waits for them, and re-layouts, local(): recent_inputs.reshape(seq, -1)  1.54 us
    concatenate x1, other arithmetic, local(): jnp.concatenate([recent_inputs[:, 1:, :], branch_x[:, None, :]], axis=1)  1.41 us
    broadcast_in_dim x1, local copies, waits for them, and re-layouts, local(): gain_mix[None]  1.29 us
    broadcast_in_dim x1, local copies, waits for them, and re-layouts, local(): gain_experts[None]  1.28 us

profile of v1, /device:TPU:0, one launch (start us, length us, event | category | flops | bytes accessed | tf_op | source)
XLA Modules:
  0.0 51.7 jit_solution(9868327520179520426)
XLA Ops:
  0.6 1.7 %copy.25.router_weight = bf16[2048,8]{1,0:T(8,128)(2,1)} copy(bf16[2048,8]{0,1:T(8,128)(2,1)} %param.30) | data formatting | bytes 65536 | tf_op args[13]
  2.4 1.5 %copy.26 = bf16[3,2,8,1024]{3,2,0,1:T(8,128)(2,1)} copy(bf16[3,2,8,1024]{3,2,1,0:T(8,128)(2,1)} %bitcast.5) | data formatting | bytes 196608 | tf_op jit(solution)/shard_map/reshape | solution.py:444
  3.9 1.3 %broadcast_in_dim.12.gain_mix = bf16[1,2048]{1,0:T(2,128)(2,1)} reshape(bf16[2048]{0:T(1024)(128)(2,1)} %param.21) | data formatting | bytes 8192 | tf_op jit(solution)/shard_map/broadcast_in_dim | solution.py:446
  5.2 1.3 %broadcast_in_dim.14.gain_experts = bf16[1,2048]{1,0:T(2,128)(2,1)} reshape(bf16[2048]{0:T(1024)(128)(2,1)} %param.29) | data formatting | bytes 8192 | tf_op jit(solution)/shard_map/broadcast_in_dim | solution.py:451
  6.5 1.4 %copy.24.routes = s32[16,2]{1,0:T(8,128)} copy(s32[16,2]{0,1:T(2,128)} %param.20) | data formatting | bytes 256 | tf_op args[3]
  7.8 0.0 copy-start
  7.8 39.4 %shard_map.184 = (bf16[16,2048]{1,0:T(8,128)(2,1)}, f32[16,1024]{1,0:T(8,128)}, bf16[16,1024]{1,0:T(8,128)(2,1)}) custom-call(bf16[16,2048]{1,0:T(8,128)(2,1)} %tokens.1, f32[16,1024]{1,0:T(8,128)} %hidden_state.1, bf16[16,3072]{1,0:T(8,128)(2,1)} %bitcast.4, s32[16,2]{1,0:T(8,128)} %copy.24.routes, bf16[1,2048]{1,0:T(2,128)(2,1)} %broadcast_in_dim.12.gain_mix, ...), custom_call_target="tpu_custom_call" | custom-call | tf_op jit(solution)/shard_map/pallas_call | solution.py:395
  47.3 0.0 copy-done
  47.3 1.4 %pad_maximum_fusion = bf16[16,3,1024]{2,0,1:T(8,128)(2,1)} fusion(bf16[16,1,1024]{2,0,1:T(8,128)(2,1)} %bitcast.6, bf16[16,2,1024]{2,0,1:T(8,128)(2,1)S(1)} %slice.3), kind=kLoop, calls=%fused_computation | loop fusion | flops 49152 | bytes 196608 | tf_op jit(solution)/shard_map/concatenate | solution.py:460
  48.7 1.5 %copy.29 = bf16[16,2048]{1,0:T(8,128)(2,1)} copy(bf16[16,2048]{1,0:T(8,128)(2,1)} %get-tuple-element.12) | data formatting | bytes 131072
  50.2 1.5 %copy.30 = f32[16,1024]{1,0:T(8,128)} copy(f32[16,1024]{1,0:T(8,128)} %get-tuple-element.13) | data formatting | bytes 131072
  (1 shorter events, 0.0 us)
Async XLA Ops:
  7.8 39.4 %copy-start = (bf16[16,3,1024]{2,0,1:T(8,128)(2,1)S(1)}, bf16[16,3,1024]{2,0,1:T(8,128)(2,1)}, u32[]{:S(2)}) copy-start(bf16[16,3,1024]{2,0,1:T(8,128)(2,1)} %param.19) | copy-start | bytes 294916

commit v2 on v1

--- a/solution.py
+++ b/solution.py
@@ -11,7 +11,7 @@
 CAP = 8
 TAPS = 4
 BITS = 3
-ORDER = (1, 4, 6, 2, 5, 7, 3)
+ORDER = (1, 4, 2, 6, 3, 5, 7)
 
 epsilon = 1e-06
 rate_scale = 8.0
@@ -23,6 +23,19 @@
 def rms_scale(values, gain):
     mean_square = jnp.mean(values * values, axis=-1, keepdims=True)
     return values * lax.rsqrt(mean_square + epsilon) * gain.astype(f32)
+
+
+def as_row(blocks):
+    values = blocks[...].astype(f32)
+    return jnp.concatenate([values[i : i + 1] for i in range(values.shape[0])], axis=1)
+
+
+def write_out(layer, hidden, branch_x, recent, layer_out, hidden_out, inputs_out):
+    layer_out[...] = layer[...]
+    hidden_out[...] = hidden[...]
+    for j in range(TAPS - 2):
+        inputs_out[j] = recent[j + 1]
+    inputs_out[TAPS - 2] = branch_x[...]
 
 
 def flip(e, k):
@@ -137,7 +150,7 @@
     branch_loads = load(w_branch_hbm, w_branch, parts)
     out_loads = load(w_out_hbm, w_out, parts)
     expert_loads = load(w_gate_hbm, w_gate, 1) + load(w_up_hbm, w_up, 1) + load(w_down_hbm, w_down, 1)
-    for copy in loads:
+    for copy in in_loads + branch_loads + out_loads:
         copy.start()
 
     def streamed(lhs, weight, copies):
@@ -154,14 +167,14 @@
         return total
 
     resid = tokens[...].astype(f32)
-    normed = rms_scale(resid, gain_mix[...]).astype(bf16)
+    normed = rms_scale(resid, as_row(gain_mix)).astype(bf16)
     branch_x = streamed(normed, w_in, in_loads).astype(bf16)
     branch_out[...] = branch_x
     rnn = branch_x.shape[1]
     taps = filter_taps[...].astype(f32)
     conv = branch_x.astype(f32) * taps[TAPS - 1 : TAPS]
     for j in range(TAPS - 1):
-        conv = conv + recent[:, j * rnn : (j + 1) * rnn].astype(f32) * taps[j : j + 1]
+        conv = conv + recent[j].astype(f32) * taps[j : j + 1]
     conv_out = conv.astype(bf16)
     width = recurrence_map.shape[1]
     blocks = rnn // width
@@ -189,28 +202,28 @@
     new_hidden = decay * hidden_state[...] + jnp.sqrt(lost) * (in_gate * conv_out.astype(f32))
     new_hidden_out[...] = new_hidden
     branch_g = streamed(normed, w_branch, branch_loads).astype(bf16).astype(f32)
+    for copy in expert_loads:
+        copy.start()
     mixed = (new_hidden * jax.nn.gelu(branch_g, approximate=True)).astype(bf16)
     after = resid + streamed(mixed, w_out, out_loads)
     after_ref[...] = after
-    expert_in = rms_scale(after, gain_experts[...]).astype(bf16)
+    expert_in = rms_scale(after, as_row(gain_experts)).astype(bf16)
 
     seq = expert_in.shape[0]
     slots = EXPERTS * CAP
-    col = lax.broadcasted_iota(jnp.int32, (seq, slots), 1)
-    first = routes[:, 0:1]
-    second = routes[:, 1:2]
-    pick0 = (col // CAP) == first
-    pick1 = (col // CAP) == second
+    row = lax.broadcasted_iota(jnp.int32, (slots, seq), 0)
+    first = routes[0:1, :]
+    second = routes[1:2, :]
+    pick0 = (row // CAP) == first
+    pick1 = (row // CAP) == second
     member = (pick0 | pick1).astype(f32)
     tri = (
-        lax.broadcasted_iota(jnp.int32, (seq, seq), 0) >= lax.broadcasted_iota(jnp.int32, (seq, seq), 1)
+        lax.broadcasted_iota(jnp.int32, (seq, seq), 0) <= lax.broadcasted_iota(jnp.int32, (seq, seq), 1)
     ).astype(f32)
-    rank = jnp.dot(tri.astype(bf16), member.astype(bf16), preferred_element_type=f32)
-    table = jnp.where(rank == (col % CAP + 1).astype(f32), member, 0.0)
-
-    dense = lax.dot_general(
-        table.astype(bf16), expert_in, (((0,), (0,)), ((), ())), preferred_element_type=f32
-    )
+    rank = jnp.dot(member.astype(bf16), tri.astype(bf16), preferred_element_type=f32)
+    table = jnp.where(rank == (row % CAP + 1).astype(f32), member, 0.0)
+
+    dense = jnp.dot(table.astype(bf16), expert_in, preferred_element_type=f32)
     packed[...] = dense.reshape(packed.shape).astype(bf16)
 
     pl.semaphore_wait(barrier, len(peers))
@@ -223,13 +236,16 @@
         sends.append(copy)
     x_blocks[0, 0, e] = packed[e]
 
-    logits = jnp.dot(expert_in, router_weight[...], preferred_element_type=f32)
-    ids = lax.broadcasted_iota(jnp.int32, logits.shape, 1)
-    l0 = jnp.sum(jnp.where(ids == first, logits, 0.0), axis=1, keepdims=True)
-    l1 = jnp.sum(jnp.where(ids == second, logits, 0.0), axis=1, keepdims=True)
+    logits = lax.dot_general(
+        router_weight[...], expert_in, (((1,), (1,)), ((), ())), preferred_element_type=f32
+    )
+    ids = lax.broadcasted_iota(jnp.int32, logits.shape, 0)
+    l0 = jnp.sum(jnp.where(ids == first, logits, 0.0), axis=0, keepdims=True)
+    l1 = jnp.sum(jnp.where(ids == second, logits, 0.0), axis=0, keepdims=True)
     share0 = jax.nn.sigmoid(l0 - l1)
     share1 = jax.nn.sigmoid(l1 - l0)
     scaled = table * (jnp.where(pick0, share0, 0.0) + jnp.where(pick1, share1, 0.0))
+    scaled = scaled.T
     high = scaled.astype(bf16)
     low = (scaled - high.astype(f32)).astype(bf16)
     combine = jnp.concatenate([high, low], axis=0)
@@ -386,18 +402,19 @@
         chips = group // 2
         rows = n * CAP
         block = EXPERTS * CAP
-        n_col = 4
+        n_col = 8
         wide = model // n_col
         dma = pltpu.SemaphoreType.DMA
         vmem = pl.BlockSpec(memory_space=pltpu.VMEM)
-        hbm = pl.BlockSpec(memory_space=pl.ANY)
+        hbm = pl.BlockSpec(memory_space=pltpu.HBM)
         far = max(chips - 1, 1)
+        recent = jnp.transpose(recent_inputs, (1, 0, 2))
         layer_out, new_hidden, branch_x = pl.pallas_call(
             functools.partial(kernel, n, n_col),
             out_shape=(
-                jax.ShapeDtypeStruct((seq, model), bf16),
-                jax.ShapeDtypeStruct((seq, rnn), f32),
-                jax.ShapeDtypeStruct((seq, rnn), bf16),
+                pltpu.VMEM((seq, model), bf16),
+                pltpu.VMEM((seq, rnn), f32),
+                pltpu.VMEM((seq, rnn), bf16),
             ),
             in_specs=[vmem] * 11 + [hbm] * 6,
             out_specs=(vmem, vmem, vmem),
@@ -436,20 +453,20 @@
                 dma((EXPERTS, n_col)),
             ],
             compiler_params=pltpu.CompilerParams(
-                collective_id=0, has_side_effects=True, vmem_limit_bytes=60 * 1024 * 1024
+                collective_id=0, has_side_effects=True, vmem_limit_bytes=61 * 1024 * 1024
             ),
         )(
             tokens,
             hidden_state,
-            recent_inputs.reshape(seq, -1),
-            routes,
-            gain_mix[None],
+            recent,
+            routes.T,
+            gain_mix.reshape(-1, 128),
             filter_taps,
             recurrence_map,
             input_map,
             decay_param[None],
-            gain_experts[None],
-            router_weight,
+            gain_experts.reshape(-1, 128),
+            router_weight.T,
             input_weight,
             branch_weight,
             output_weight,
@@ -457,8 +474,18 @@
             expert_up,
             expert_down,
         )
-        new_inputs = jnp.concatenate([recent_inputs[:, 1:, :], branch_x[:, None, :]], axis=1)
-        return (layer_out, new_hidden, new_inputs)
+        layer_out, new_hidden, new_inputs = pl.pallas_call(
+            write_out,
+            out_shape=(
+                jax.ShapeDtypeStruct((seq, model), bf16),
+                jax.ShapeDtypeStruct((seq, rnn), f32),
+                jax.ShapeDtypeStruct(recent.shape, bf16),
+            ),
+            in_specs=[vmem] * 4,
+            out_specs=(vmem, vmem, vmem),
+            compiler_params=pltpu.CompilerParams(vmem_limit_bytes=4 * 1024 * 1024),
+        )(layer_out, new_hidden, branch_x, recent)
+        return (layer_out, new_hidden, jnp.transpose(new_inputs, (1, 0, 2)))
 
     placed = (
         P("ep", None),

time: 52.1 us -> 42 us (0.81)
  local copies, waits for them, and re-layouts: 10.2 us -> 0.01 us
  Pallas kernels: 39.4 us -> 41.2 us
  other arithmetic: 1.41 us -> 0 us
    unnamed x6 -> x2, local copies, waits for them, and re-layouts: 6.05 us -> 0.01 us
    broadcast_in_dim x2 -> x0, local copies, waits for them, and re-layouts: 2.57 us -> none  [the longest x1 1.29 us: local(): gain_mix[None]]
    pallas_call x1 -> x2, Pallas kernels: 39.4 us -> 41.2 us  [the longest x1 40.5 us: local(): pl.pallas_call(functools.partial(kernel, n, n_col), out_shape=(pltpu.VMEM...]
    reshape x1 -> x0, local copies, waits for them, and re-layouts: 1.54 us -> none  [local(): recent_inputs.reshape(seq, -1)]
    concatenate x1 -> x0, other arithmetic: 1.41 us -> none  [local(): jnp.concatenate([recent_inputs[:, 1:, :], branch_x[:, None, :]], axis=1)]
where the time goes in v2:
time: 42 us; the launch traced here: 41.9 us
  Pallas kernels  41.2 us (98%)
  between operations  0.66 us (2%)
    pallas_call x1, Pallas kernels, local(): pl.pallas_call(functools.partial(kernel, n, n_col), out_shape=(pltpu.VMEM...  40.5 us

profile of v2, /device:TPU:0, one launch (start us, length us, event | category | flops | bytes accessed | tf_op | source)
XLA Modules:
  0.0 41.9 jit_solution(17406556422175410905)
XLA Ops:
  0.6 0.0 copy-start
  0.6 40.5 %shard_map.184 = (bf16[16,2048]{1,0:T(8,128)(2,1)S(1)}, f32[16,1024]{1,0:T(8,128)S(1)}, bf16[16,1024]{1,0:T(8,128)(2,1)S(1)}) custom-call(bf16[16,2048]{1,0:T(8,128)(2,1)} %tokens.1, f32[16,1024]{1,0:T(8,128)} %hidden_state.1, bf16[3,16,1024]{2,1,0:T(8,128)(2,1)} %bitcast.7, s32[2,16]{1,0:T(2,128)} %bitcast.13, bf16[16,128]{1,0:T(8,128)(2,1)} %bitcast.10, ...), custom_call_target="tpu_custom_call" | custom-call | tf_op jit(solution)/shard_map/pallas_call | solution.py:412
  41.2 0.0 copy-done
  41.2 0.7 %shard_map.185 = (bf16[16,2048]{1,0:T(8,128)(2,1)}, f32[16,1024]{1,0:T(8,128)}, bf16[3,16,1024]{2,1,0:T(8,128)(2,1)}) custom-call(bf16[16,2048]{1,0:T(8,128)(2,1)S(1)} %get-tuple-element.9.layer, f32[16,1024]{1,0:T(8,128)S(1)} %get-tuple-element.10.hidden, bf16[16,1024]{1,0:T(8,128)(2,1)S(1)} %get-tuple-element.11.branch_x, bf16[3,16,1024]{2,1,0:T(8,128)(2,1)S(1)} %bitcast.8), custom_call_target="tpu_custom_call" | custom-call | tf_op jit(solution)/shard_map/pallas_call | solution.py:477
Async XLA Ops:
  0.6 40.5 %copy-start = (bf16[16,3,1024]{2,0,1:T(8,128)(2,1)S(1)}, bf16[16,3,1024]{2,0,1:T(8,128)(2,1)}, u32[]{:S(2)}) copy-start(bf16[16,3,1024]{2,0,1:T(8,128)(2,1)} %param.19) | copy-start | bytes 294916

commit v3 on v2

--- a/solution.py
+++ b/solution.py
@@ -51,6 +51,26 @@
 def kernel(
     n,
     n_col,
+    tokens_hbm,
+    hidden_state_hbm,
+    recent_hbm,
+    routes_hbm,
+    gain_mix_hbm,
+    filter_taps_hbm,
+    recurrence_map_hbm,
+    input_map_hbm,
+    decay_param_hbm,
+    gain_experts_hbm,
+    router_weight_hbm,
+    w_in_hbm,
+    w_branch_hbm,
+    w_out_hbm,
+    w_gate_hbm,
+    w_up_hbm,
+    w_down_hbm,
+    layer_out,
+    new_hidden_out,
+    branch_out,
     tokens,
     hidden_state,
     recent,
@@ -62,15 +82,6 @@
     decay_param,
     gain_experts,
     router_weight,
-    w_in_hbm,
-    w_branch_hbm,
-    w_out_hbm,
-    w_gate_hbm,
-    w_up_hbm,
-    w_down_hbm,
-    layer_out,
-    new_hidden_out,
-    branch_out,
     w_in,
     w_branch,
     w_out,
@@ -103,6 +114,7 @@
     b_r,
     c_s,
     c_r,
+    small_sem,
 ):
     me = lax.axis_index("ep")
     group = n // EXPERTS
@@ -134,6 +146,22 @@
             barrier, inc=1, device_id=(dev,), device_id_type=pl.DeviceIdType.MESH
         )
 
+    small = [
+        (tokens_hbm, tokens),
+        (gain_mix_hbm, gain_mix),
+        (hidden_state_hbm, hidden_state),
+        (recent_hbm, recent),
+        (routes_hbm, routes),
+        (filter_taps_hbm, filter_taps),
+        (recurrence_map_hbm, recurrence_map),
+        (input_map_hbm, input_map),
+        (decay_param_hbm, decay_param),
+        (gain_experts_hbm, gain_experts),
+        (router_weight_hbm, router_weight),
+    ]
+    small = [pltpu.make_async_copy(src, dst, small_sem.at[i]) for i, (src, dst) in enumerate(small)]
+    for copy in small:
+        copy.start()
     parts = 4
     loads = []
 
@@ -166,10 +194,14 @@
             total = part if total is None else total + part
         return total
 
+    for copy in small[:2]:
+        copy.wait()
     resid = tokens[...].astype(f32)
     normed = rms_scale(resid, as_row(gain_mix)).astype(bf16)
     branch_x = streamed(normed, w_in, in_loads).astype(bf16)
     branch_out[...] = branch_x
+    for copy in small[2:]:
+        copy.wait()
     rnn = branch_x.shape[1]
     taps = filter_taps[...].astype(f32)
     conv = branch_x.astype(f32) * taps[TAPS - 1 : TAPS]
@@ -402,13 +434,26 @@
         chips = group // 2
         rows = n * CAP
         block = EXPERTS * CAP
-        n_col = 8
+        n_col = 4
         wide = model // n_col
         dma = pltpu.SemaphoreType.DMA
         vmem = pl.BlockSpec(memory_space=pltpu.VMEM)
         hbm = pl.BlockSpec(memory_space=pltpu.HBM)
         far = max(chips - 1, 1)
         recent = jnp.transpose(recent_inputs, (1, 0, 2))
+        small = (
+            tokens,
+            hidden_state,
+            recent,
+            routes.T,
+            gain_mix.reshape(-1, 128),
+            filter_taps,
+            recurrence_map,
+            input_map,
+            decay_param[None],
+            gain_experts.reshape(-1, 128),
+            router_weight.T,
+        )
         layer_out, new_hidden, branch_x = pl.pallas_call(
             functools.partial(kernel, n, n_col),
             out_shape=(
@@ -416,9 +461,10 @@
                 pltpu.VMEM((seq, rnn), f32),
                 pltpu.VMEM((seq, rnn), bf16),
             ),
-            in_specs=[vmem] * 11 + [hbm] * 6,
+            in_specs=[hbm] * 17,
             out_specs=(vmem, vmem, vmem),
-            scratch_shapes=[
+            scratch_shapes=[pltpu.VMEM(x.shape, x.dtype) for x in small]
+            + [
                 pltpu.VMEM(input_weight.shape, bf16),
                 pltpu.VMEM(branch_weight.shape, bf16),
                 pltpu.VMEM(output_weight.shape, bf16),
@@ -451,22 +497,13 @@
                 dma((far, n_col)),
                 dma((EXPERTS, n_col)),
                 dma((EXPERTS, n_col)),
+                dma((len(small),)),
             ],
             compiler_params=pltpu.CompilerParams(
                 collective_id=0, has_side_effects=True, vmem_limit_bytes=61 * 1024 * 1024
             ),
         )(
-            tokens,
-            hidden_state,
-            recent,
-            routes.T,
-            gain_mix.reshape(-1, 128),
-            filter_taps,
-            recurrence_map,
-            input_map,
-            decay_param[None],
-            gain_experts.reshape(-1, 128),
-            router_weight.T,
+            *small,
             input_weight,
             branch_weight,
             output_weight,

time: 42 us -> 39.6 us (0.943)
  Pallas kernels: 41.2 us -> 38.8 us
    pallas_call x1, Pallas kernels: 40.5 us -> 38.1 us  [local(): pl.pallas_call(functools.partial(kernel, n, n_col), out_shape=(pltpu.VMEM...]
where the time goes in v3:
time: 39.6 us; the launch traced here: 39.5 us
  Pallas kernels  38.8 us (98%)
  between operations  0.66 us (2%)
    pallas_call x1, Pallas kernels, local(): pl.pallas_call(functools.partial(kernel, n, n_col), out_shape=(pltpu.VMEM...  38.1 us

profile of v3, /device:TPU:0, one launch (start us, length us, event | category | flops | bytes accessed | tf_op | source)
XLA Modules:
  0.0 39.5 jit_solution(14447287974037655565)
XLA Ops:
  0.6 0.0 copy-start
  0.6 38.1 %shard_map.184 = (bf16[16,2048]{1,0:T(8,128)(2,1)S(1)}, f32[16,1024]{1,0:T(8,128)S(1)}, bf16[16,1024]{1,0:T(8,128)(2,1)S(1)}) custom-call(bf16[16,2048]{1,0:T(8,128)(2,1)} %tokens_hbm.1, f32[16,1024]{1,0:T(8,128)} %hidden_state_hbm.1, bf16[3,16,1024]{2,1,0:T(8,128)(2,1)} %bitcast.7, s32[2,16]{1,0:T(2,128)} %bitcast.13, bf16[16,128]{1,0:T(8,128)(2,1)} %bitcast.10, ...), custom_call_target="tpu_custom_call" | custom-call | tf_op jit(solution)/shard_map/pallas_call | solution.py:457
  38.7 0.0 copy-done
  38.8 0.7 %shard_map.185 = (bf16[16,2048]{1,0:T(8,128)(2,1)}, f32[16,1024]{1,0:T(8,128)}, bf16[3,16,1024]{2,1,0:T(8,128)(2,1)}) custom-call(bf16[16,2048]{1,0:T(8,128)(2,1)S(1)} %get-tuple-element.9.layer, f32[16,1024]{1,0:T(8,128)S(1)} %get-tuple-element.10.hidden, bf16[16,1024]{1,0:T(8,128)(2,1)S(1)} %get-tuple-element.11.branch_x, bf16[3,16,1024]{2,1,0:T(8,128)(2,1)S(1)} %bitcast.8), custom_call_target="tpu_custom_call" | custom-call | tf_op jit(solution)/shard_map/pallas_call | solution.py:514
Async XLA Ops:
  0.6 38.1 %copy-start = (bf16[16,3,1024]{2,0,1:T(8,128)(2,1)S(1)}, bf16[16,3,1024]{2,0,1:T(8,128)(2,1)}, u32[]{:S(2)}) copy-start(bf16[16,3,1024]{2,0,1:T(8,128)(2,1)} %param.19) | copy-start | bytes 294916
